TPU v7x, 32 devices: a whole 2x2x4 slice. The times are simulated.
32 devices in a mesh: sp: 8 (over z, y), tp: 4 (over x, core).
Axes of the slice: x: 2, y: 2, z: 4, core: 2. Of those that a mesh axis runs over, the one named last changes fastest.
Arguments:
- hidden_states: bfloat16 [4096, 4096], P('sp', 'tp'), may hold values from -6 to 6
- pre_gain: float32 [2, 4096], replicated, may hold values from 0.1 to 1.9
- post_gain: float32 [2, 4096], P(None, 'tp'), may hold values from 0.1 to 1.9
- w_value: bfloat16 [2, 4096, 2048], P(None, 'sp', 'tp'), may hold values from -0.09375 to 0.09375
- w_outer: bfloat16 [2, 4096, 2048], P(None, 'sp', 'tp'), may hold values from -0.09375 to 0.09375
- w_inner: bfloat16 [2, 4096, 2048], P(None, 'sp', 'tp'), may hold values from -0.09375 to 0.09375
- taps: float32 [2, 3, 2048], P(None, None, 'tp'), may hold values from -3 to 3
- w_out: bfloat16 [2, 2048, 4096], P(None, 'tp', 'sp'), as said below
Outputs:
- final_states: bfloat16 [4096, 4096], P('sp', 'tp')
Inputs may be any that keep to these rules, and one draw needn't show every extreme that they name: `w_out`: independent entries; the columns fall into 8 groups of 512 consecutive columns, each group with its own scale.
All inputs are finite; a program needn't handle non-finite values.
Results may differ from a plain program's by a relative error of at most 0.024.
Values may be sent and summed in bfloat16 or wider, within the bound.
A program may use at most 128 MiB of HBM per device.

v0:
```python
import jax
import jax.numpy as jnp
from jax import lax
from jax.sharding import PartitionSpec as P

D = 4096
eps = 1e-06


def passed_along(value, axis, by):
    size = lax.axis_size(axis)
    pairs = [(i, i + by) for i in range(size) if 0 <= i + by < size]
    return lax.ppermute(value, axis, pairs)


def local(hidden_states, pre_gain, post_gain, w_value, w_outer, w_inner, taps, w_out):
    current = hidden_states
    layers = w_value.shape[0]
    whole_value, whole_outer, whole_inner, whole_out = (
        lax.all_gather(w_value, "sp", axis=1, tiled=True),
        lax.all_gather(w_outer, "sp", axis=1, tiled=True),
        lax.all_gather(w_inner, "sp", axis=1, tiled=True),
        lax.all_gather(w_out, "sp", axis=2, tiled=True),
    )
    for layer_index in range(layers):
        gathered = lax.all_gather(current, "tp", axis=1, tiled=True)
        widened = gathered.astype(jnp.float32)
        normed = (
            widened
            * lax.rsqrt(jnp.mean(widened * widened, axis=1, keepdims=True) + eps)
            * pre_gain[layer_index]
        ).astype(jnp.bfloat16)
        value_proj = jnp.dot(normed, whole_value[layer_index], preferred_element_type=jnp.float32)
        outer_proj = jnp.dot(normed, whole_outer[layer_index], preferred_element_type=jnp.float32)
        inner_proj = jnp.dot(normed, whole_inner[layer_index], preferred_element_type=jnp.float32)
        gated_input = (inner_proj * value_proj).astype(jnp.bfloat16)
        before = passed_along(gated_input[-2:], "sp", 1)
        extended = jnp.concatenate([before, gated_input], axis=0).astype(jnp.float32)
        length = gated_input.shape[0]
        kernel = taps[layer_index]
        convolved = (
            extended[0:length] * kernel[0]
            + extended[1 : length + 1] * kernel[1]
            + extended[2 : length + 2] * kernel[2]
        )
        conv_out = (outer_proj * convolved).astype(jnp.bfloat16)
        partial_terms = jnp.dot(
            conv_out, whole_out[layer_index], preferred_element_type=jnp.float32
        )
        mixed = lax.psum_scatter(
            partial_terms.astype(jnp.bfloat16), "tp", scatter_dimension=1, tiled=True
        ).astype(jnp.float32)
        power = lax.psum(jnp.sum(mixed * mixed, axis=1), "tp")
        rescale = lax.rsqrt(power / D + eps)
        current = (
            current.astype(jnp.float32) + mixed * rescale[:, None] * post_gain[layer_index]
        ).astype(jnp.bfloat16)
    return current


def solution(mesh):
    placed = (
        P("sp", "tp"),
        P(),
        P(None, "tp"),
        P(None, "sp", "tp"),
        P(None, "sp", "tp"),
        P(None, "sp", "tp"),
        P(None, None, "tp"),
        P(None, "tp", "sp"),
    )
    return jax.shard_map(
        local, mesh=mesh, in_specs=placed, out_specs=P("sp", "tp"), check_vma=False
    )
```

profile of v0, /device:TPU:0, one launch (start us, length us, event | category | flops | bytes accessed | tf_op | source)
XLA Modules:
  0.0 729.6 jit_solution(7224380522898905791)
XLA Ops:
  6.5 0.7 all-gather.7.cloned.1.call-update
  7.3 0.7 all-gather.13.cloned.1.call-update
  8.1 0.7 all-gather.11.cloned.1.call-update
  10.0 36.1 %all-gather.7.cloned.1.call-done = bf16[512,4096]{1,0:T(8,128)(2,1)} async-done(((bf16[512,1024]{1,0:T(8,128)(2,1)}), bf16[512,4096]{1,0:T(8,128)(2,1)}) %all-gather.7.cloned.1.call-update) | async-done | bytes 4194320 | tf_op jit(solution)/shard_map/all_gather | solution.py:26
  46.1 3.1 fusion
  49.2 123.6 %all-gather.13.cloned.1.call-done = bf16[2,4096,512]{2,1,0:T(8,128)(2,1)} async-done(((bf16[2,512,512]{2,1,0:T(8,128)(2,1)}), bf16[2,4096,512]{2,1,0:T(8,128)(2,1)}) %all-gather.13.cloned.1.call-update) | async-done | bytes 8388624 | tf_op jit(solution)/shard_map/all_gather | solution.py:20
  172.8 5.8 fusion.9
  178.6 119.0 %all-gather.11.cloned.1.call-done = bf16[2,4096,512]{2,1,0:T(8,128)(2,1)} async-done(((bf16[2,512,512]{2,1,0:T(8,128)(2,1)}), bf16[2,4096,512]{2,1,0:T(8,128)(2,1)}) %all-gather.11.cloned.1.call-update) | async-done | bytes 8388624 | tf_op jit(solution)/shard_map/all_gather | solution.py:22
  297.6 5.8 fusion.26
  303.5 2.5 collective-permute-start
  306.0 1.3 collective-permute-done
  307.4 114.9 %all-gather.9.cloned.1.call-done = bf16[2,4096,512]{2,1,0:T(8,128)(2,1)} async-done(((bf16[2,512,512]{2,1,0:T(8,128)(2,1)}), bf16[2,4096,512]{2,1,0:T(8,128)(2,1)}) %all-gather.9.cloned.1.call-update) | async-done | bytes 8388624 | tf_op jit(solution)/shard_map/all_gather | solution.py:21
  422.4 6.0 fusion.27
  428.4 119.0 %all-gather.15.cloned.1.call-done = bf16[2,512,4096]{2,1,0:T(8,128)(2,1)} async-done(((bf16[2,512,512]{2,1,0:T(8,128)(2,1)}), bf16[2,512,4096]{2,1,0:T(8,128)(2,1)}) %all-gather.15.cloned.1.call-update) | async-done | bytes 8388624 | tf_op jit(solution)/shard_map/all_gather | solution.py:23
  547.4 6.7 convolution_convert_fusion.1
  554.8 42.1 %reduce-scatter.3.cloned.1.call-done = bf16[512,1024]{1,0:T(8,128)(2,1)} async-done(((bf16[512,4096]{1,0:T(8,128)(2,1)}), bf16[512,1024]{1,0:T(8,128)(2,1)}) %reduce-scatter.3.cloned.1.call-update) | async-done | bytes 1048592 | tf_op jit(solution)/shard_map/reduce_scatter | solution.py:50
  596.8 1.5 fusion.12
  598.3 5.8 psum.14
  604.1 2.6 fusion.15
  607.0 35.0 %all-gather.17.cloned.1.call-done = bf16[512,4096]{1,0:T(8,128)(2,1)} async-done(((bf16[512,1024]{1,0:T(8,128)(2,1)}), bf16[512,4096]{1,0:T(8,128)(2,1)}) %all-gather.17.cloned.1.call-update) | async-done | bytes 4194320 | tf_op jit(solution)/shard_map/all_gather | solution.py:26
  642.0 3.2 fusion.3
  645.4 4.7 fusion.6
  650.2 4.7 fusion.24
  655.0 3.4 collective-permute-start.1
  658.3 1.3 collective-permute-done.1
  659.8 2.6 fusion.25
  662.4 0.7 slice-done.1
  663.2 4.3 convolution_convert_fusion
  667.5 45.4 %reduce-scatter.5.cloned.1.call-done = bf16[512,1024]{1,0:T(8,128)(2,1)} async-done(((bf16[512,4096]{1,0:T(8,128)(2,1)}), bf16[512,1024]{1,0:T(8,128)(2,1)}) %reduce-scatter.5.cloned.1.call-update) | async-done | bytes 1048592 | tf_op jit(solution)/shard_map/reduce_scatter | solution.py:50
  712.9 1.5 fusion.16
  714.4 5.8 psum.15
  720.1 2.6 fusion.19
  (45 shorter events, 2.8 us)
Async XLA Ops:
  6.5 3.4 copy-start.3
  6.5 39.6 %all-gather.7.cloned.1.call-start = ((), (), s32[]{:S(2)}) async-start(), calls=%async_computation.2 | async-start | bytes 5242880 | tf_op jit(solution)/shard_map/all_gather | solution.py:26
  7.3 165.5 %all-gather.13.cloned.1.call-start = ((), (), s32[]{:S(2)}) async-start(), calls=%async_computation.5 | async-start | bytes 9437184 | tf_op jit(solution)/shard_map/all_gather | solution.py:20
  8.0 289.6 %all-gather.11.cloned.1.call-start = ((), (), s32[]{:S(2)}) async-start(), calls=%async_computation.4 | async-start | bytes 9437184 | tf_op jit(solution)/shard_map/all_gather | solution.py:22
  8.7 413.6 %all-gather.9.cloned.1.call-start = ((), (), s32[]{:S(2)}) async-start(), calls=%async_computation.3 | async-start | bytes 9437184 | tf_op jit(solution)/shard_map/all_gather | solution.py:21
  9.3 538.1 %all-gather.15.cloned.1.call-start = ((), (), s32[]{:S(2)}) async-start(), calls=%async_computation.6 | async-start | bytes 9437184 | tf_op jit(solution)/shard_map/all_gather | solution.py:23
  9.9 586.9 %reduce-scatter.3.cloned.1.call-start = ((), (), s32[]{:S(2)}) async-start(), calls=%async_computation.7 | async-start | bytes 5242880 | tf_op jit(solution)/shard_map/reduce_scatter | solution.py:50
  178.6 127.4 %copy-start.4 = (f32[2,3,512]{2,0,1:T(2,128)S(1)}, f32[2,3,512]{2,0,1:T(2,128)}, u32[]{:S(2)}) copy-start(f32[2,3,512]{2,0,1:T(2,128)} %param.14) | copy-start | bytes 36868
  303.5 3.8 collective-permute-start
  554.1 0.7 copy-start.5
  554.1 50.0 %copy-start.2 = (bf16[512,1024]{1,0:T(8,128)(2,1)S(1)}, bf16[512,1024]{1,0:T(8,128)(2,1)}, u32[]{:S(2)}) copy-start(bf16[512,1024]{1,0:T(8,128)(2,1)} %param.8) | copy-start | bytes 3145732
  554.1 87.9 %all-gather.17.cloned.1.call-start = ((), (), s32[]{:S(2)}) async-start(), calls=%async_computation.8 | async-start | bytes 5242880 | tf_op jit(solution)/shard_map/all_gather | solution.py:26
  606.8 106.1 %reduce-scatter.5.cloned.1.call-start = ((), (), s32[]{:S(2)}) async-start(), calls=%async_computation.9 | async-start | bytes 5242880 | tf_op jit(solution)/shard_map/reduce_scatter | solution.py:50
  642.0 3.4 copy-start.1
  645.4 14.4 %slice-start.2 = ((s8[8388608]{0:T(1024)(128)(4,1)}), s8[4194304]{0:T(1024)(128)(4,1)S(1)}, s32[]{:S(2)}) async-start(s8[8388608]{0:T(1024)(128)(4,1)} %bitcast.68), calls=%async_computation.12 | async-start | bytes 8388608
  650.2 9.6 %slice-start.3 = ((s8[8388608]{0:T(1024)(128)(4,1)}), s8[4194304]{0:T(1024)(128)(4,1)S(1)}, s32[]{:S(2)}) async-start(s8[8388608]{0:T(1024)(128)(4,1)} %bitcast.68), calls=%async_computation.13 | async-start | bytes 8388608
  655.0 4.7 collective-permute-start.1
  659.6 2.8 slice-start
  659.8 3.3 slice-start.1
  667.5 52.7 %copy-start = (bf16[512,1024]{1,0:T(8,128)(2,1)S(1)}, bf16[512,1024]{1,0:T(8,128)(2,1)}, u32[]{:S(2)}) copy-start(bf16[512,1024]{1,0:T(8,128)(2,1)} %fusion.15) | copy-start | bytes 3145732
Sparse Core Ops, SparseCore 0:
  8.9 37.1 all-gather.6
  48.3 124.4 all-gather.12
  175.0 122.6 all-gather.10
  299.7 122.6 all-gather.8
  424.2 123.1 all-gather.14
  554.2 42.5 reduce-scatter.2
  606.9 35.0 all-gather.16
  667.6 45.2 reduce-scatter.4
where the time goes:
time: 730 us
  waiting for transfers between devices  641 us (88%)
  matrix products  40.7 us (6%)
  other arithmetic  14.9 us (2%)
  between operations  13.7 us (2%)
  blocking collectives  11.5 us (2%)
    all_gather x1, waiting for transfers between devices, local(): lax.all_gather(w_value, 'sp', axis=1, tiled=True)  124 us
    all_gather x1, waiting for transfers between devices, local(): lax.all_gather(w_out, 'sp', axis=2, tiled=True)  119 us
    all_gather x1, waiting for transfers between devices, local(): lax.all_gather(w_inner, 'sp', axis=1, tiled=True)  119 us
    all_gather x1, waiting for transfers between devices, local(): lax.all_gather(w_outer, 'sp', axis=1, tiled=True)  115 us
    reduce_scatter x2, waiting for transfers between devices, local(): lax.psum_scatter(partial_terms.astype(jnp.bfloat16), 'tp', scatter_dimens...  87.4 us
    all_gather x2, waiting for transfers between devices, local(): gathered = lax.all_gather(current, 'tp', axis=1, tiled=True)  71.1 us
  transfers between devices with their start and end apart: 10, of which 10 were waited for; matrix products, arithmetic and copies ran while one was open for 3% of the time, Pallas kernels for 0%

commit v1 on v0

--- a/solution.py
+++ b/solution.py
@@ -1,3 +1,4 @@
+import functools
 import jax
 import jax.numpy as jnp
 from jax import lax
@@ -5,6 +6,14 @@
 
 D = 4096
 eps = 1e-06
+
+
+def set_sizes(raw, which_dim):
+    r1 = lax.all_gather(raw, axis_name="sp")
+    return jnp.concatenate(r1, axis=which_dim)
+
+
+lift_halves = functools.partial(set_sizes, which_dim=1)
 
 
 def passed_along(value, axis, by):
@@ -17,7 +26,7 @@
     current = hidden_states
     layers = w_value.shape[0]
     whole_value, whole_outer, whole_inner, whole_out = (
-        lax.all_gather(w_value, "sp", axis=1, tiled=True),
+        lift_halves(w_value),
         lax.all_gather(w_outer, "sp", axis=1, tiled=True),
         lax.all_gather(w_inner, "sp", axis=1, tiled=True),
         lax.all_gather(w_out, "sp", axis=2, tiled=True),

time: 730 us -> 730 us (level)
  no operation moved by 1% of the time
where the time goes in v1:
time: 730 us; the launch traced here: 729 us
  waiting for transfers between devices  638 us (87%)
  matrix products  37.2 us (5%)
  other arithmetic  14.9 us (2%)
  between operations  13.7 us (2%)
  blocking collectives  11.5 us (2%)
  local copies, waits for them, and re-layouts  7.81 us (1%)
    all_gather x1, waiting for transfers between devices, set_sizes(): r1 = lax.all_gather(raw, axis_name='sp')  124 us
    all_gather x1, waiting for transfers between devices, local(): lax.all_gather(w_out, 'sp', axis=2, tiled=True)  119 us
    all_gather x1, waiting for transfers between devices, local(): lax.all_gather(w_inner, 'sp', axis=1, tiled=True)  116 us
    all_gather x1, waiting for transfers between devices, local(): lax.all_gather(w_outer, 'sp', axis=1, tiled=True)  115 us
    reduce_scatter x2, waiting for transfers between devices, local(): lax.psum_scatter(partial_terms.astype(jnp.bfloat16), 'tp', scatter_dimens...  87.4 us
    all_gather x2, waiting for transfers between devices, local(): gathered = lax.all_gather(current, 'tp', axis=1, tiled=True)  71.1 us
  transfers between devices with their start and end apart: 10, of which 10 were waited for; matrix products, arithmetic and copies ran while one was open for 3% of the time, Pallas kernels for 0%

profile of v1, /device:TPU:0, one launch (start us, length us, event | category | flops | bytes accessed | tf_op | source)
XLA Modules:
  0.0 729.5 jit_solution(13753367195559894327)
XLA Ops:
  6.5 0.7 all-gather.8.cloned.1.call-update
  10.0 36.1 %all-gather.8.cloned.1.call-done = bf16[512,4096]{1,0:T(8,128)(2,1)} async-done(((bf16[512,1024]{1,0:T(8,128)(2,1)}), bf16[512,4096]{1,0:T(8,128)(2,1)}) %all-gather.8.cloned.1.call-update) | async-done | bytes 4194320 | tf_op jit(solution)/shard_map/all_gather | solution.py:35
  46.1 3.1 fusion
  49.2 123.5 %all-gather.18.cloned.1.call-done = bf16[16,512,512]{2,1,0:T(8,128)(2,1)} async-done(((bf16[2,512,512]{2,1,0:T(8,128)(2,1)}), bf16[16,512,512]{2,1,0:T(8,128)(2,1)}) %all-gather.18.cloned.1.call-update) | async-done | bytes 8388624 | tf_op jit(solution)/shard_map/all_gather | solution.py:12
  172.7 5.3 fusion.38
  178.0 0.9 copy-done.1
  178.9 2.4 fusion.34
  181.3 116.3 %all-gather.12.cloned.1.call-done = bf16[2,4096,512]{2,1,0:T(8,128)(2,1)} async-done(((bf16[2,512,512]{2,1,0:T(8,128)(2,1)}), bf16[2,4096,512]{2,1,0:T(8,128)(2,1)}) %all-gather.12.cloned.1.call-update) | async-done | bytes 8388624 | tf_op jit(solution)/shard_map/all_gather | solution.py:31
  297.6 5.8 fusion.24
  303.5 2.5 collective-permute-start
  306.0 1.3 collective-permute-done
  307.4 114.9 %all-gather.10.cloned.1.call-done = bf16[2,4096,512]{2,1,0:T(8,128)(2,1)} async-done(((bf16[2,512,512]{2,1,0:T(8,128)(2,1)}), bf16[2,4096,512]{2,1,0:T(8,128)(2,1)}) %all-gather.10.cloned.1.call-update) | async-done | bytes 8388624 | tf_op jit(solution)/shard_map/all_gather | solution.py:30
  422.3 6.0 fusion.25
  428.3 119.0 %all-gather.14.cloned.1.call-done = bf16[2,512,4096]{2,1,0:T(8,128)(2,1)} async-done(((bf16[2,512,512]{2,1,0:T(8,128)(2,1)}), bf16[2,512,4096]{2,1,0:T(8,128)(2,1)}) %all-gather.14.cloned.1.call-update) | async-done | bytes 8388624 | tf_op jit(solution)/shard_map/all_gather | solution.py:32
  547.4 6.6 convolution_convert_fusion.1
  554.6 42.1 %reduce-scatter.3.cloned.1.call-done = bf16[512,1024]{1,0:T(8,128)(2,1)} async-done(((bf16[512,4096]{1,0:T(8,128)(2,1)}), bf16[512,1024]{1,0:T(8,128)(2,1)}) %reduce-scatter.3.cloned.1.call-update) | async-done | bytes 1048592 | tf_op jit(solution)/shard_map/reduce_scatter | solution.py:59
  596.7 1.5 fusion.10
  598.2 5.8 psum.14
  604.0 2.6 fusion.13
  606.9 35.0 %all-gather.16.cloned.1.call-done = bf16[512,4096]{1,0:T(8,128)(2,1)} async-done(((bf16[512,1024]{1,0:T(8,128)(2,1)}), bf16[512,4096]{1,0:T(8,128)(2,1)}) %all-gather.16.cloned.1.call-update) | async-done | bytes 4194320 | tf_op jit(solution)/shard_map/all_gather | solution.py:35
  641.8 3.2 fusion.3
  645.3 4.7 fusion.30
  650.1 4.7 fusion.22
  654.8 3.4 collective-permute-start.1
  658.2 1.3 collective-permute-done.1
  659.7 2.6 fusion.23
  662.3 0.7 slice-done.1
  663.0 4.3 convolution_convert_fusion
  667.3 45.4 %reduce-scatter.5.cloned.1.call-done = bf16[512,1024]{1,0:T(8,128)(2,1)} async-done(((bf16[512,4096]{1,0:T(8,128)(2,1)}), bf16[512,1024]{1,0:T(8,128)(2,1)}) %reduce-scatter.5.cloned.1.call-update) | async-done | bytes 1048592 | tf_op jit(solution)/shard_map/reduce_scatter | solution.py:59
  712.7 1.5 fusion.14
  714.2 5.8 psum.15
  720.0 2.6 fusion.17
  (48 shorter events, 4.2 us)
Async XLA Ops:
  6.5 3.4 copy-start.4
  6.5 39.6 %all-gather.8.cloned.1.call-start = ((), (), s32[]{:S(2)}) async-start(), calls=%async_computation.2 | async-start | bytes 5242880 | tf_op jit(solution)/shard_map/all_gather | solution.py:35
  7.3 165.5 %all-gather.18.cloned.1.call-start = ((), (), s32[]{:S(2)}) async-start(), calls=%async_computation.9 | async-start | bytes 9437184 | tf_op jit(solution)/shard_map/all_gather | solution.py:12
  8.0 289.6 %all-gather.12.cloned.1.call-start = ((), (), s32[]{:S(2)}) async-start(), calls=%async_computation.4 | async-start | bytes 9437184 | tf_op jit(solution)/shard_map/all_gather | solution.py:31
  8.7 413.6 %all-gather.10.cloned.1.call-start = ((), (), s32[]{:S(2)}) async-start(), calls=%async_computation.3 | async-start | bytes 9437184 | tf_op jit(solution)/shard_map/all_gather | solution.py:30
  9.3 538.0 %all-gather.14.cloned.1.call-start = ((), (), s32[]{:S(2)}) async-start(), calls=%async_computation.5 | async-start | bytes 9437184 | tf_op jit(solution)/shard_map/all_gather | solution.py:32
  9.9 586.8 %reduce-scatter.3.cloned.1.call-start = ((), (), s32[]{:S(2)}) async-start(), calls=%async_computation.6 | async-start | bytes 5242880 | tf_op jit(solution)/shard_map/reduce_scatter | solution.py:59
  172.7 6.2 copy-start.1
  181.3 124.6 %copy-start.5 = (f32[2,3,512]{2,0,1:T(2,128)S(1)}, f32[2,3,512]{2,0,1:T(2,128)}, u32[]{:S(2)}) copy-start(f32[2,3,512]{2,0,1:T(2,128)} %param.14) | copy-start | bytes 36868
  303.5 3.8 collective-permute-start
  553.9 0.7 copy-start.6
  553.9 50.0 %copy-start.3 = (bf16[512,1024]{1,0:T(8,128)(2,1)S(1)}, bf16[512,1024]{1,0:T(8,128)(2,1)}, u32[]{:S(2)}) copy-start(bf16[512,1024]{1,0:T(8,128)(2,1)} %param.8) | copy-start | bytes 3145732
  553.9 87.9 %all-gather.16.cloned.1.call-start = ((), (), s32[]{:S(2)}) async-start(), calls=%async_computation.7 | async-start | bytes 5242880 | tf_op jit(solution)/shard_map/all_gather | solution.py:35
  606.6 106.1 %reduce-scatter.5.cloned.1.call-start = ((), (), s32[]{:S(2)}) async-start(), calls=%async_computation.8 | async-start | bytes 5242880 | tf_op jit(solution)/shard_map/reduce_scatter | solution.py:59
  641.8 3.4 copy-start.2
  645.3 14.4 %slice-start.2 = ((s8[8388608]{0:T(1024)(128)(4,1)}), s8[4194304]{0:T(1024)(128)(4,1)S(1)}, s32[]{:S(2)}) async-start(s8[8388608]{0:T(1024)(128)(4,1)} %bitcast.72), calls=%async_computation.12 | async-start | bytes 8388608
  650.0 9.6 %slice-start.3 = ((s8[8388608]{0:T(1024)(128)(4,1)}), s8[4194304]{0:T(1024)(128)(4,1)S(1)}, s32[]{:S(2)}) async-start(s8[8388608]{0:T(1024)(128)(4,1)} %bitcast.72), calls=%async_computation.13 | async-start | bytes 8388608
  654.8 4.7 collective-permute-start.1
  659.5 2.8 slice-start
  659.7 3.3 slice-start.1
  667.3 52.7 %copy-start = (bf16[512,1024]{1,0:T(8,128)(2,1)S(1)}, bf16[512,1024]{1,0:T(8,128)(2,1)}, u32[]{:S(2)}) copy-start(bf16[512,1024]{1,0:T(8,128)(2,1)} %fusion.13) | copy-start | bytes 3145732
Sparse Core Ops, SparseCore 0:
  8.9 37.1 all-gather.7
  48.2 124.4 all-gather.17
  174.9 122.6 all-gather.11
  299.6 122.6 all-gather.9
  424.2 123.1 all-gather.13
  554.1 42.5 reduce-scatter.2
  606.7 35.0 all-gather.15
  667.4 45.2 reduce-scatter.4
